TPU v7x, 32 devices: a whole 2x2x4 slice. The times are simulated.
32 devices in a mesh: sp: 8 (over z, x), tp: 4 (over y, core).
Axes of the slice: x: 2, y: 2, z: 4, core: 2. Of those that a mesh axis runs over, the one named last changes fastest.
Arguments:
- residual_in: bfloat16 [1536, 2048], P('sp', 'tp'), may hold values from -6 to 6
- query_rows: bfloat16 [1536, 1024], P('sp', 'tp'), may hold values from -8 to 8
- key_rows: bfloat16 [1536, 1024], P('sp', 'tp'), may hold values from -8 to 8
- value_rows: bfloat16 [1536, 1024], P('sp', 'tp'), may hold values from -6 to 6
- map_weight: float32 [16], P('tp'), may hold values from 0.3 to 0.8
- head_gain: float32 [64], replicated, may hold values from 0.1 to 1.9
- out_proj: bfloat16 [1024, 2048], P(None, 'tp'), may hold values from -0.1875 to 0.1875
- norm_gain: float32 [2048], replicated, may hold values from 0.1 to 1.9
- route_ids: int32 [1536, 2], P('sp'), may hold values from 0 to 7, all different within a row; in each aligned block of 192 rows (0 to 191, 192 to 383, ...) at most 60 rows name the same one
- route_weights: float32 [1536, 2], P('sp'), may hold values from 0.2 to 1.2
- expert_gate: bfloat16 [8, 1024, 2048], P('sp', 'tp'), may hold values from -0.125 to 0.125
- expert_up: bfloat16 [8, 1024, 2048], P('sp', 'tp'), may hold values from -0.125 to 0.125
- expert_down: bfloat16 [8, 1024, 2048], P('sp', None, 'tp'), may hold values from -0.1875 to 0.1875
- shared_gate: bfloat16 [1024, 2048], P('tp'), may hold values from -0.125 to 0.125
- shared_up: bfloat16 [1024, 2048], P('tp'), may hold values from -0.125 to 0.125
- shared_down: bfloat16 [1024, 2048], P(None, 'tp'), may hold values from -0.1875 to 0.1875
Outputs:
- mixed_out: bfloat16 [1536, 2048], P('sp', 'tp')
Inputs may be any that keep to these rules, and one draw needn't show every extreme that they name: `route_ids`: each row names 2 different experts. Among the rows held by one index of sp no expert is named more than 60 times, and in every draw some expert is named exactly 60 times by the rows of some index of sp.
All inputs are finite; a program needn't handle non-finite values.
Results may differ from a plain program's by a relative error of at most 0.0095.
Values may be sent and summed in bfloat16 or wider, within the bound.
No kernel may reach another device: no remote copies, remote signals or barrier semaphores. Data moves between devices by JAX's collectives and lax.ppermute only.
A program may use at most 64 MiB of HBM per device.

v0:
```python
import jax
import jax.numpy as jnp
from jax import lax
from jax.sharding import PartitionSpec as P

epsilon = 1e-06
masked_score = -1e30


def rms_scale(values, gain_vec):
    squares = jnp.mean(values * values, axis=-1, keepdims=True)
    return values * lax.rsqrt(squares + epsilon) * gain_vec


def block_slots(route_block, experts_all, capacity):
    flat_ids = route_block.reshape(-1)
    one_hot = (flat_ids[:, None] == jnp.arange(experts_all, dtype=jnp.int32)[None, :]).astype(
        jnp.int32
    )
    earlier = jnp.cumsum(one_hot, axis=0) - one_hot
    position = jnp.sum(earlier * one_hot, axis=1)
    return (flat_ids * capacity + position).reshape(route_block.shape)


def body(
    residual_in,
    query_rows,
    key_rows,
    value_rows,
    map_weight,
    head_gain,
    out_proj,
    norm_gain,
    route_ids,
    route_weights,
    expert_gate,
    expert_up,
    expert_down,
    shared_gate,
    shared_up,
    shared_down,
):
    seq_dev = residual_in.shape[0]
    col_dev = residual_in.shape[1]
    heads_here = map_weight.shape[0]
    head_dim = head_gain.shape[0]
    half_dim = head_dim // 2
    topk_count = route_ids.shape[1]
    exp_here = expert_gate.shape[0]
    experts_all = exp_here * lax.axis_size("sp")
    capacity = 5 * seq_dev * topk_count // (4 * experts_all)
    score_scale = half_dim ** (-0.5)
    query_pos = lax.axis_index("sp") * seq_dev + jnp.arange(seq_dev, dtype=jnp.int32)
    query_heads = query_rows.reshape(seq_dev, heads_here, 2, half_dim)
    key_piece = lax.all_gather(key_rows, "sp", axis=0, tiled=True)
    value_piece = lax.all_gather(value_rows, "sp", axis=0, tiled=True)
    piece_len = key_piece.shape[0]
    key_heads = key_piece.reshape(piece_len, heads_here, 2, half_dim)
    value_heads = value_piece.reshape(piece_len, heads_here, head_dim)
    scores = (
        jnp.einsum("qhmd,khmd->mhqk", query_heads, key_heads, preferred_element_type=jnp.float32)
        * score_scale
    )
    key_pos = jnp.arange(piece_len, dtype=jnp.int32)
    visible = key_pos[None, :] <= query_pos[:, None]
    scores = jnp.where(visible, scores, masked_score)
    run_max = jnp.full((2, heads_here, seq_dev), masked_score, jnp.float32)
    new_max = jnp.maximum(run_max, jnp.max(scores, axis=-1))
    expo = jnp.where(visible, jnp.exp(scores - new_max[..., None]), 0.0)
    new_sum = jnp.sum(expo, axis=-1)
    product = jnp.einsum(
        "mhqk,khd->mhqd", expo.astype(jnp.bfloat16), value_heads, preferred_element_type=jnp.float32
    )
    summed = product / new_sum[..., None]
    diff_out = summed[0] - map_weight[:, None, None] * summed[1]
    head_out = rms_scale(diff_out, head_gain).astype(jnp.bfloat16)
    head_out = jnp.transpose(head_out, (1, 0, 2)).reshape(seq_dev, heads_here * head_dim)
    attn = jnp.dot(
        lax.all_gather(head_out, "tp", axis=1, tiled=True),
        out_proj,
        preferred_element_type=jnp.float32,
    )
    hidden_state = (residual_in.astype(jnp.float32) + attn).astype(jnp.bfloat16)
    full_rows = lax.all_gather(hidden_state, "tp", axis=1, tiled=True)
    normed = rms_scale(full_rows.astype(jnp.float32), norm_gain).astype(jnp.bfloat16)
    shared_gate_part = jnp.einsum(
        "rd,fd->rf", normed, shared_gate, preferred_element_type=jnp.float32
    )
    shared_up_part = jnp.einsum("rd,fd->rf", normed, shared_up, preferred_element_type=jnp.float32)
    shared_hidden = (jax.nn.silu(shared_gate_part) * shared_up_part).astype(jnp.bfloat16)
    slot_ids = block_slots(route_ids, experts_all, capacity)
    token_of = jnp.repeat(jnp.arange(seq_dev, dtype=jnp.int32), topk_count)
    slot_token = (
        jnp.full((experts_all * capacity,), seq_dev, jnp.int32)
        .at[slot_ids.reshape(-1)]
        .set(token_of)
    )
    own_cols = lax.dynamic_slice_in_dim(normed, lax.axis_index("tp") * col_dev, col_dev, 1)
    padded = jnp.concatenate([own_cols, jnp.zeros((1, col_dev), jnp.bfloat16)], axis=0)
    outgoing = jnp.take(padded, slot_token, axis=0).reshape(experts_all, capacity, col_dev)
    arrived = lax.all_to_all(outgoing, "sp", split_axis=0, concat_axis=1, tiled=True)
    arrived_rows = arrived.shape[1]
    pieces = lax.all_gather(arrived, "tp", axis=2, tiled=True)
    gate_add = jnp.einsum("erd,efd->erf", pieces, expert_gate, preferred_element_type=jnp.float32)
    up_add = jnp.einsum("erd,efd->erf", pieces, expert_up, preferred_element_type=jnp.float32)
    expert_hidden = (jax.nn.silu(gate_add) * up_add).astype(jnp.bfloat16)
    expert_flat = expert_hidden.reshape(exp_here * arrived_rows, expert_hidden.shape[2])
    pieces = (
        lax.all_gather(shared_hidden, "tp", axis=1, tiled=True),
        lax.all_gather(expert_flat, "tp", axis=1, tiled=True),
    )
    piece_width = pieces[0].shape[1]
    routed_piece = pieces[1].reshape(exp_here, arrived_rows, piece_width)
    shared_add = jnp.dot(pieces[0], shared_down, preferred_element_type=jnp.float32)
    expert_add = jnp.einsum(
        "erf,efd->erd", routed_piece, expert_down, preferred_element_type=jnp.float32
    )
    returned_rows = lax.all_to_all(
        expert_add.astype(jnp.bfloat16), "sp", split_axis=1, concat_axis=0, tiled=True
    )
    returned_flat = returned_rows.reshape(experts_all * capacity, col_dev)
    picked = (
        jnp.take(returned_flat, slot_ids.reshape(-1), axis=0)
        .reshape(seq_dev, topk_count, col_dev)
        .astype(jnp.float32)
    )
    routed = jnp.sum(picked * route_weights[:, :, None], axis=1)
    return (hidden_state.astype(jnp.float32) + shared_add + routed).astype(jnp.bfloat16)


def solution(mesh):
    in_specs = (
        P("sp", "tp"),
        P("sp", "tp"),
        P("sp", "tp"),
        P("sp", "tp"),
        P("tp"),
        P(),
        P(None, "tp"),
        P(),
        P("sp", None),
        P("sp", None),
        P("sp", "tp", None),
        P("sp", "tp", None),
        P("sp", None, "tp"),
        P("tp", None),
        P("tp", None),
        P(None, "tp"),
    )
    out_specs = P("sp", "tp")
    return jax.shard_map(body, mesh=mesh, in_specs=in_specs, out_specs=out_specs, check_vma=False)
```

profile of v0, /device:TPU:0, one launch (start us, length us, event | category | flops | bytes accessed | tf_op | source)
XLA Modules:
  0.0 206.6 jit_solution(2744693201549045714)
XLA Ops:
  6.5 0.9 copy.68
  7.4 0.1 eq.26
  7.6 0.1 reshape.160
  7.7 0.7 broadcast_multiply_fusion
  8.4 0.8 reduce-window.6
  9.3 0.2 slice_reduce_fusion
  9.6 0.1 mul.124
  9.8 0.1 reshape.188
  10.1 2.9 %scatter_custom_fusion = s32[480]{0:T(512)S(1)} fusion(s32[384]{0:T(512)S(1)} %fusion.40, s32[384]{0:T(512)S(1)} %reshape.188, s32[]{:T(128)} %constant.26.clone.1), kind=kCustom, calls=%fused_computation.66 | custom fusion | bytes 1924 | tf_op jit(solution)/shard_map/scatter | solution.py:96
  13.0 0.2 iota_compare_fusion
  13.3 34.1 %all_gather.21 = bf16[1536,256]{1,0:T(8,128)(2,1)S(1)} all-gather(bf16[192,256]{1,0:T(8,128)(2,1)} %param.18), channel_id=1, replica_groups=mesh['sp'=8,'tp'=4] {'sp'}, dimensions={0}, use_global_device_ids=true | all-gather | bytes 884736 | tf_op jit(solution)/shard_map/all_gather | solution.py:55
  47.4 0.3 copy.61
  47.6 1.0 copy.60
  48.6 1.9 fusion
  50.5 4.4 %fusion.1 = (f32[2,4,192]{2,1,0:T(4,128)S(1)}, bf16[2,4,192,1536]{3,2,1,0:T(8,128)(2,1)}) fusion(f32[2,4,192,1536]{3,2,1,0:T(8,128)S(1)} %get-tuple-element.8, f32[2,4,192]{2,1,0:T(4,128)S(1)} %broadcast_maximum_fusion, pred[192,1536]{1,0:T(8,128)(4,1)S(1)} %iota_compare_fusion), kind=kLoop, calls=%fused_computation.6 | loop fusion | flops 14154240 | bytes 14462976 | tf_op jit(solution)/shard_map/reduce_sum | solution.py:70
  55.0 32.1 %all_gather.22 = bf16[1536,256]{1,0:T(8,128)(2,1)S(1)} all-gather(bf16[192,256]{1,0:T(8,128)(2,1)S(1)} %copy-done.2), channel_id=1, replica_groups=mesh['sp'=8,'tp'=4] {'sp'}, dimensions={0}, use_global_device_ids=true | all-gather | bytes 884736 | tf_op jit(solution)/shard_map/all_gather | solution.py:56
  87.1 0.3 copy.64
  87.4 4.0 %fusion.29 = f32[2,4,192,64]{2,3,0,1:T(8,128)S(1)} fusion(bf16[1536,4,64,1]{0,2,3,1:T(8,128)(2,1)S(1)} %bitcast.84, bf16[2,4,192,1536]{3,2,1,0:T(8,128)(2,1)} %get-tuple-element.6, f32[2,4,192]{2,0,1:T(2,128)S(1)} %copy.66), kind=kOutput, calls=%fused_computation.35 | convolution fusion | flops 302088192 | bytes 5904384 | tf_op jit(solution)/shard_map/mhqk,khd->mhqd/dot_general | solution.py:71
  91.7 7.2 %all_gather.23 = bf16[192,1024]{0,1:T(8,128)(2,1)S(1)} all-gather(bf16[192,256]{0,1:T(8,128)(2,1)S(1)} %bitcast.85), channel_id=1, replica_groups=mesh['sp'=8,'tp'=4] {'tp'}, dimensions={1}, use_global_device_ids=true | all-gather | bytes 491520 | tf_op jit(solution)/shard_map/all_gather | solution.py:79
  98.9 1.1 fusion.23
  100.0 8.9 %all_gather.24 = bf16[192,2048]{1,0:T(8,128)(2,1)S(1)} all-gather(bf16[192,512]{1,0:T(8,128)(2,1)} %fusion.23), channel_id=1, replica_groups=mesh['sp'=8,'tp'=4] {'tp'}, dimensions={1}, use_global_device_ids=true | all-gather | bytes 983040 | tf_op jit(solution)/shard_map/all_gather | solution.py:84
  108.9 0.2 fusion.9
  109.2 0.3 fusion.11
  109.5 2.1 %gather_fusion = bf16[480,512]{1,0:T(8,128)(2,1)S(1)} fusion(bf16[193,512]{1,0:T(8,128)(2,1)S(1)} %concatenate.3, s32[1024]{0:T(1024)S(1)} %pad_clamp_fusion.1), kind=kCustom, calls=%fused_computation | custom fusion | bytes 984960 | tf_op jit(solution)/shard_map/jit(_take)/gather | solution.py:100
  111.8 0.1 broadcast_select_fusion.1
  112.0 20.3 %all_to_all.21 = bf16[8,60,512]{2,1,0:T(8,128)(2,1)S(1)} all-to-all(bf16[8,60,512]{2,1,0:T(8,128)(2,1)S(1)} %broadcast_select_fusion.1), channel_id=1, replica_groups=mesh['sp'=8,'tp'=4] {'sp'}, dimensions={0} | all-to-all | bytes 983040 | tf_op jit(solution)/shard_map/all_to_all | solution.py:101
  132.3 0.9 all_to_all.7
  133.2 0.1 reduce_sum.53
  133.4 20.1 %all-gather.2.cloned.1.call-done = bf16[1,480,2048]{2,1,0:T(8,128)(2,1)} async-done(((bf16[1,480,512]{2,1,0:T(8,128)(2,1)}), bf16[1,480,2048]{2,1,0:T(8,128)(2,1)}) %all-gather.2.cloned.1.call-update) | async-done | bytes 1966096 | tf_op jit(solution)/shard_map/all_gather | solution.py:103
  153.6 2.7 %fusion.7 = f32[480,256]{1,0:T(8,128)S(1)} fusion(bf16[1,480,2048]{2,1,0:T(8,128)(2,1)} %all-gather.2.cloned.1.call-done, bf16[1,256,2048]{2,1,0:T(8,128)(2,1)} %param.26), kind=kOutput, calls=%fused_computation.12 | convolution fusion | flops 503316480 | bytes 3506176 | tf_op jit(solution)/shard_map/erd,efd->erf/dot_general | solution.py:104
  156.3 0.7 fusion.20
  157.0 9.8 %all_gather.27 = bf16[480,1024]{1,0:T(8,128)(2,1)S(1)} all-gather(bf16[480,256]{1,0:T(8,128)(2,1)S(1)} %fusion.20), channel_id=1, replica_groups=mesh['sp'=8,'tp'=4] {'tp'}, dimensions={1}, use_global_device_ids=true | all-gather | bytes 1228800 | tf_op jit(solution)/shard_map/all_gather | solution.py:110
  166.8 0.7 fusion.15
  167.5 0.8 copy.95
  168.3 0.6 broadcast.119
  168.9 3.7 %reduce.4 = bf16[480,512]{1,0:T(8,128)(2,1)S(1)} reduce(bf16[480,1,512]{2,1,0:T(2,128)(2,1)S(1)} %bitcast.81, bf16[]{:T(256)} %broadcast.119), dimensions={1}, to_apply=%bitcast.78.reduce_sub_computation | reduce | bytes 983042
  172.5 1.0 reshape.198
  173.5 5.5 %all-to-all-start.1 = ((bf16[8,2,15360]{2,1,0:T(2,128)(2,1)}), bf16[8,2,15360]{2,1,0:T(2,128)(2,1)S(1)}, u32[]{:S(2)}, u32[]{:S(2)}) async-start(bf16[8,2,15360]{2,1,0:T(2,128)(2,1)} %reshape.198), calls=%async_computation.1 | async-start | bytes 983040 | tf_op jit(solution)/shard_map/all_to_all | solution.py:118
  179.0 0.2 copy.71
  179.3 1.7 fusion.43
  181.1 1.7 fusion.25
  182.8 6.3 %all_gather.25 = bf16[192,1024]{1,0:T(8,128)(2,1)S(1)} all-gather(bf16[192,256]{1,0:T(8,128)(2,1)S(1)} %fusion.25), channel_id=1, replica_groups=mesh['sp'=8,'tp'=4] {'tp'}, dimensions={1}, use_global_device_ids=true | all-gather | bytes 491520 | tf_op jit(solution)/shard_map/all_gather | solution.py:109
  189.1 4.2 %all-to-all-done.1 = bf16[8,2,15360]{2,1,0:T(2,128)(2,1)S(1)} async-done(((bf16[8,2,15360]{2,1,0:T(2,128)(2,1)}), bf16[8,2,15360]{2,1,0:T(2,128)(2,1)S(1)}, u32[]{:S(2)}, u32[]{:S(2)}) %all-to-all-start.1) | async-done | bytes 491552 | tf_op jit(solution)/shard_map/all_to_all | solution.py:118
  193.3 0.4 reshape.199
  193.9 2.1 gather_fusion.1
  195.9 0.2 gather.15
  196.1 1.6 multiply_reduce_fusion
  197.7 2.0 fusion.24
  (51 shorter events, 1.2 us)
Async XLA Ops:
  6.5 160.3 %copy-start = (bf16[1,1024,512]{2,1,0:T(8,128)(2,1)S(1)}, bf16[1,1024,512]{2,1,0:T(8,128)(2,1)}, u32[]{:S(2)}) copy-start(bf16[1,1024,512]{2,1,0:T(8,128)(2,1)} %param.28) | copy-start | bytes 3145732
  6.5 147.0 %all-gather.2.cloned.1.call-start = ((), (), s32[]{:S(2)}) async-start(), calls=%async_computation.2 | async-start | bytes 2457600 | tf_op jit(solution)/shard_map/all_gather | solution.py:103
  50.5 4.5 %copy-start.2 = (bf16[192,256]{1,0:T(8,128)(2,1)S(1)}, bf16[192,256]{1,0:T(8,128)(2,1)}, u32[]{:S(2)}) copy-start(bf16[192,256]{1,0:T(8,128)(2,1)} %param.19) | copy-start | bytes 294916
  87.4 4.1 %copy-start.5 = (f32[4]{0:T(128)S(1)}, f32[4]{0:T(128)}, u32[]{:S(2)}) copy-start(f32[4]{0:T(128)} %param.20) | copy-start | bytes 52
  87.4 4.2 %copy-start.7 = (f32[64]{0:T(128)S(1)}, f32[64]{0:T(128)}, u32[]{:S(2)}) copy-start(f32[64]{0:T(128)} %param.21) | copy-start | bytes 772
  87.4 11.6 %copy-start.9 = (bf16[1024,512]{1,0:T(8,128)(2,1)S(1)}, bf16[1024,512]{1,0:T(8,128)(2,1)}, u32[]{:S(2)}) copy-start(bf16[1024,512]{1,0:T(8,128)(2,1)} %param.22) | copy-start | bytes 3145732
  87.4 11.5 %copy-start.11 = (bf16[192,512]{1,0:T(8,128)(2,1)S(1)}, bf16[192,512]{1,0:T(8,128)(2,1)}, u32[]{:S(2)}) copy-start(bf16[192,512]{1,0:T(8,128)(2,1)} %param.16) | copy-start | bytes 589828
  91.4 17.7 %copy-start.4 = (f32[2048]{0:T(1024)S(1)}, f32[2048]{0:T(1024)}, u32[]{:S(2)}) copy-start(f32[2048]{0:T(1024)} %param.23) | copy-start | bytes 24580
  133.3 22.9 %copy-start.10 = (bf16[1,256,2048]{2,1,0:T(8,128)(2,1)S(1)}, bf16[1,256,2048]{2,1,0:T(8,128)(2,1)}, u32[]{:S(2)}) copy-start(bf16[1,256,2048]{2,1,0:T(8,128)(2,1)} %param.27) | copy-start | bytes 3145732
  153.6 2.7 %copy-start.8 = (bf16[1,480,2048]{2,1,0:T(8,128)(2,1)S(1)}, bf16[1,480,2048]{2,1,0:T(8,128)(2,1)}, u32[]{:S(2)}) copy-start(bf16[1,480,2048]{2,1,0:T(8,128)(2,1)} %all-gather.2.cloned.1.call-done) | copy-start | bytes 5898244
  157.0 22.0 %copy-start.3 = (s32[192,2]{0,1:T(2,128)S(1)}, s32[192,2]{0,1:T(2,128)}, u32[]{:S(2)}) copy-start(s32[192,2]{0,1:T(2,128)} %param.24) | copy-start | bytes 4612
  157.0 22.2 %copy-start.6 = (f32[192,2]{0,1:T(2,128)S(1)}, f32[192,2]{0,1:T(2,128)}, u32[]{:S(2)}) copy-start(f32[192,2]{0,1:T(2,128)} %param.25) | copy-start | bytes 4612
  173.5 19.8 %all-to-all-start.1 = ((bf16[8,2,15360]{2,1,0:T(2,128)(2,1)}), bf16[8,2,15360]{2,1,0:T(2,128)(2,1)S(1)}, u32[]{:S(2)}, u32[]{:S(2)}) async-start(bf16[8,2,15360]{2,1,0:T(2,128)(2,1)} %reshape.198), calls=%async_computation.1 | async-start | bytes 983040 | tf_op jit(solution)/shard_map/all_to_all | solution.py:118
  193.9 3.9 %copy-start.1 = (bf16[1024,512]{1,0:T(8,128)(2,1)S(1)}, bf16[1024,512]{1,0:T(8,128)(2,1)}, u32[]{:S(2)}) copy-start(bf16[1024,512]{1,0:T(8,128)(2,1)} %param.31) | copy-start | bytes 3145732
Sparse Core Ops, SparseCore 0:
  133.3 20.2 all-gather.1
where the time goes:
time: 207 us
  blocking collectives  119 us (57%)
  waiting for transfers between devices  24.4 us (12%)
  matrix products  16.5 us (8%)
  local copies, waits for them, and re-layouts  15.1 us (7%)
  between operations  13.8 us (7%)
  other arithmetic  12.6 us (6%)
  starting transfers between devices  5.51 us (3%)
    all_gather x1, blocking collectives, body(): key_piece = lax.all_gather(key_rows, 'sp', axis=0, tiled=True)  34.1 us
    all_gather x1, blocking collectives, body(): value_piece = lax.all_gather(value_rows, 'sp', axis=0, tiled=True)  32.1 us
    all_to_all x1, blocking collectives, body(): lax.all_to_all(outgoing, 'sp', split_axis=0, concat_axis=1, tiled=True)  20.3 us
    all_gather x1, waiting for transfers between devices, body(): pieces = lax.all_gather(arrived, 'tp', axis=2, tiled=True)  20.1 us
    all_gather x1, blocking collectives, body(): lax.all_gather(expert_flat, 'tp', axis=1, tiled=True)  9.84 us
    all_gather x1, blocking collectives, body(): full_rows = lax.all_gather(hidden_state, 'tp', axis=1, tiled=True)  8.9 us
    all_gather x1, blocking collectives, body(): lax.all_gather(head_out, 'tp', axis=1, tiled=True)  7.21 us
    all_gather x1, blocking collectives, body(): lax.all_gather(shared_hidden, 'tp', axis=1, tiled=True)  6.29 us
  transfers between devices with their start and end apart: 2, of which 2 were waited for; matrix products, arithmetic and copies ran while one was open for 2% of the time, Pallas kernels for 0%

commit v1 on v0

--- a/solution.py
+++ b/solution.py
@@ -98,7 +98,9 @@
     own_cols = lax.dynamic_slice_in_dim(normed, lax.axis_index("tp") * col_dev, col_dev, 1)
     padded = jnp.concatenate([own_cols, jnp.zeros((1, col_dev), jnp.bfloat16)], axis=0)
     outgoing = jnp.take(padded, slot_token, axis=0).reshape(experts_all, capacity, col_dev)
-    arrived = lax.all_to_all(outgoing, "sp", split_axis=0, concat_axis=1, tiled=True)
+    parts = jnp.split(outgoing, lax.axis_size("sp"), axis=0)
+    received = lax.all_to_all(jnp.stack(parts), "sp", 0, 0)
+    arrived = jnp.concatenate(received, axis=1)
     arrived_rows = arrived.shape[1]
     pieces = lax.all_gather(arrived, "tp", axis=2, tiled=True)
     gate_add = jnp.einsum("erd,efd->erf", pieces, expert_gate, preferred_element_type=jnp.float32)

time: 207 us -> 208 us (level)
    unnamed x31 -> x36, local copies, waits for them, and re-layouts: 4.14 us -> 4.22 us
where the time goes in v1:
time: 208 us
  blocking collectives  119 us (57%)
  waiting for transfers between devices  24.4 us (12%)
  matrix products  17.7 us (9%)
  local copies, waits for them, and re-layouts  15 us (7%)
  between operations  13.9 us (7%)
  other arithmetic  12.5 us (6%)
  starting transfers between devices  5.51 us (3%)
    all_gather x1, blocking collectives, body(): key_piece = lax.all_gather(key_rows, 'sp', axis=0, tiled=True)  34.1 us
    all_gather x1, blocking collectives, body(): value_piece = lax.all_gather(value_rows, 'sp', axis=0, tiled=True)  32.1 us
    all_to_all x1, blocking collectives, body(): received = lax.all_to_all(jnp.stack(parts), 'sp', 0, 0)  20.3 us
    all_gather x1, waiting for transfers between devices, body(): pieces = lax.all_gather(arrived, 'tp', axis=2, tiled=True)  20.2 us
    all_gather x1, blocking collectives, body(): lax.all_gather(expert_flat, 'tp', axis=1, tiled=True)  9.84 us
    all_gather x1, blocking collectives, body(): full_rows = lax.all_gather(hidden_state, 'tp', axis=1, tiled=True)  8.9 us
    all_gather x1, blocking collectives, body(): lax.all_gather(head_out, 'tp', axis=1, tiled=True)  7.21 us
    all_gather x1, blocking collectives, body(): lax.all_gather(shared_hidden, 'tp', axis=1, tiled=True)  6.29 us
  transfers between devices with their start and end apart: 2, of which 2 were waited for; matrix products, arithmetic and copies ran while one was open for 2% of the time, Pallas kernels for 0%

profile of v1, /device:TPU:0, one launch (start us, length us, event | category | flops | bytes accessed | tf_op | source)
XLA Modules:
  0.0 207.8 jit_solution(3338166483786695574)
XLA Ops:
  6.5 0.9 copy.68
  7.4 0.1 eq.26
  7.6 0.1 reshape.170
  7.7 0.7 broadcast_multiply_fusion
  8.4 0.8 reduce-window.6
  9.3 0.2 slice_reduce_fusion
  9.6 0.1 mul.124
  9.8 0.1 reshape.199
  10.1 2.9 %scatter_custom_fusion = s32[480]{0:T(512)S(1)} fusion(s32[384]{0:T(512)S(1)} %fusion.48, s32[384]{0:T(512)S(1)} %reshape.199, s32[]{:T(128)} %constant.26.clone.1), kind=kCustom, calls=%fused_computation.82 | custom fusion | bytes 1924 | tf_op jit(solution)/shard_map/scatter | solution.py:96
  13.0 0.2 iota_compare_fusion
  13.3 34.1 %all_gather.21 = bf16[1536,256]{1,0:T(8,128)(2,1)S(1)} all-gather(bf16[192,256]{1,0:T(8,128)(2,1)} %param.18), channel_id=1, replica_groups=mesh['sp'=8,'tp'=4] {'sp'}, dimensions={0}, use_global_device_ids=true | all-gather | bytes 884736 | tf_op jit(solution)/shard_map/all_gather | solution.py:55
  47.4 0.3 copy.61
  47.6 1.0 copy.60
  48.6 1.9 fusion
  50.5 4.4 %fusion.1 = (f32[2,4,192]{2,1,0:T(4,128)S(1)}, bf16[2,4,192,1536]{3,2,1,0:T(8,128)(2,1)}) fusion(f32[2,4,192,1536]{3,2,1,0:T(8,128)S(1)} %get-tuple-element.8, f32[2,4,192]{2,1,0:T(4,128)S(1)} %broadcast_maximum_fusion, pred[192,1536]{1,0:T(8,128)(4,1)S(1)} %iota_compare_fusion), kind=kLoop, calls=%fused_computation.6 | loop fusion | flops 14154240 | bytes 14462976 | tf_op jit(solution)/shard_map/reduce_sum | solution.py:70
  55.0 32.1 %all_gather.22 = bf16[1536,256]{1,0:T(8,128)(2,1)S(1)} all-gather(bf16[192,256]{1,0:T(8,128)(2,1)S(1)} %copy-done.2), channel_id=1, replica_groups=mesh['sp'=8,'tp'=4] {'sp'}, dimensions={0}, use_global_device_ids=true | all-gather | bytes 884736 | tf_op jit(solution)/shard_map/all_gather | solution.py:56
  87.1 0.3 copy.64
  87.4 4.0 %fusion.29 = f32[2,4,192,64]{2,3,0,1:T(8,128)S(1)} fusion(bf16[1536,4,64,1]{0,2,3,1:T(8,128)(2,1)S(1)} %bitcast.116, bf16[2,4,192,1536]{3,2,1,0:T(8,128)(2,1)} %get-tuple-element.6, f32[2,4,192]{2,0,1:T(2,128)S(1)} %copy.66), kind=kOutput, calls=%fused_computation.35 | convolution fusion | flops 302088192 | bytes 5904384 | tf_op jit(solution)/shard_map/mhqk,khd->mhqd/dot_general | solution.py:71
  91.5 0.1 multiply_reduce_fusion.1
  91.7 7.2 %all_gather.23 = bf16[192,1024]{0,1:T(8,128)(2,1)S(1)} all-gather(bf16[192,256]{0,1:T(8,128)(2,1)S(1)} %bitcast.117), channel_id=1, replica_groups=mesh['sp'=8,'tp'=4] {'tp'}, dimensions={1}, use_global_device_ids=true | all-gather | bytes 491520 | tf_op jit(solution)/shard_map/all_gather | solution.py:79
  98.9 1.1 fusion.23
  100.0 8.9 %all_gather.24 = bf16[192,2048]{1,0:T(8,128)(2,1)S(1)} all-gather(bf16[192,512]{1,0:T(8,128)(2,1)} %fusion.23), channel_id=1, replica_groups=mesh['sp'=8,'tp'=4] {'tp'}, dimensions={1}, use_global_device_ids=true | all-gather | bytes 983040 | tf_op jit(solution)/shard_map/all_gather | solution.py:84
  108.9 0.2 fusion.9
  109.2 0.3 fusion.11
  109.5 2.1 %gather_fusion = bf16[480,512]{1,0:T(8,128)(2,1)S(1)} fusion(bf16[193,512]{1,0:T(8,128)(2,1)S(1)} %concatenate.3, s32[1024]{0:T(1024)S(1)} %get-tuple-element.10), kind=kCustom, calls=%fused_computation | custom fusion | bytes 984960 | tf_op jit(solution)/shard_map/jit(_take)/gather | solution.py:100
  111.9 20.3 %all_to_all.14 = bf16[8,1,60,512]{3,2,1,0:T(8,128)(2,1)S(1)} all-to-all(bf16[8,1,60,512]{3,2,1,0:T(8,128)(2,1)S(1)} %fusion.37), channel_id=1, replica_groups=mesh['sp'=8,'tp'=4] {'sp'}, dimensions={0} | all-to-all | bytes 983040 | tf_op jit(solution)/shard_map/all_to_all | solution.py:102
  132.2 0.9 reshape.173
  133.2 0.1 reduce_sum.53
  133.4 20.2 %all-gather.2.cloned.1.call-done = bf16[1,480,2048]{2,1,0:T(8,128)(2,1)} async-done(((bf16[1,480,512]{2,1,0:T(8,128)(2,1)}), bf16[1,480,2048]{2,1,0:T(8,128)(2,1)}) %all-gather.2.cloned.1.call-update) | async-done | bytes 1966096 | tf_op jit(solution)/shard_map/all_gather | solution.py:105
  153.5 2.7 %fusion.7 = f32[480,256]{1,0:T(8,128)S(1)} fusion(bf16[1,480,2048]{2,1,0:T(8,128)(2,1)} %all-gather.2.cloned.1.call-done, bf16[1,256,2048]{2,1,0:T(8,128)(2,1)} %param.26), kind=kOutput, calls=%fused_computation.12 | convolution fusion | flops 503316480 | bytes 3506176 | tf_op jit(solution)/shard_map/erd,efd->erf/dot_general | solution.py:106
  156.2 1.9 fusion.20
  158.2 9.8 %all_gather.27 = bf16[480,1024]{1,0:T(8,128)(2,1)S(1)} all-gather(bf16[480,256]{1,0:T(8,128)(2,1)S(1)} %fusion.20), channel_id=1, replica_groups=mesh['sp'=8,'tp'=4] {'tp'}, dimensions={1}, use_global_device_ids=true | all-gather | bytes 1228800 | tf_op jit(solution)/shard_map/all_gather | solution.py:112
  168.0 0.7 fusion.15
  168.7 0.8 copy.95
  169.5 0.6 broadcast.117
  170.1 3.7 %reduce.4 = bf16[480,512]{1,0:T(8,128)(2,1)S(1)} reduce(bf16[480,1,512]{2,1,0:T(2,128)(2,1)S(1)} %bitcast.113, bf16[]{:T(256)} %broadcast.117), dimensions={1}, to_apply=%bitcast.110.reduce_sub_computation | reduce | bytes 983042
  173.7 1.0 reshape.209
  174.7 5.5 %all-to-all-start.1 = ((bf16[8,2,15360]{2,1,0:T(2,128)(2,1)}), bf16[8,2,15360]{2,1,0:T(2,128)(2,1)S(1)}, u32[]{:S(2)}, u32[]{:S(2)}) async-start(bf16[8,2,15360]{2,1,0:T(2,128)(2,1)} %reshape.209), calls=%async_computation.1 | async-start | bytes 983040 | tf_op jit(solution)/shard_map/all_to_all | solution.py:120
  180.2 0.2 copy.71
  180.5 1.7 fusion.51
  182.3 1.7 fusion.25
  184.0 6.3 %all_gather.25 = bf16[192,1024]{1,0:T(8,128)(2,1)S(1)} all-gather(bf16[192,256]{1,0:T(8,128)(2,1)S(1)} %fusion.25), channel_id=1, replica_groups=mesh['sp'=8,'tp'=4] {'tp'}, dimensions={1}, use_global_device_ids=true | all-gather | bytes 491520 | tf_op jit(solution)/shard_map/all_gather | solution.py:111
  190.3 4.2 %all-to-all-done.1 = bf16[8,2,15360]{2,1,0:T(2,128)(2,1)S(1)} async-done(((bf16[8,2,15360]{2,1,0:T(2,128)(2,1)}), bf16[8,2,15360]{2,1,0:T(2,128)(2,1)S(1)}, u32[]{:S(2)}, u32[]{:S(2)}) %all-to-all-start.1) | async-done | bytes 491552 | tf_op jit(solution)/shard_map/all_to_all | solution.py:120
  194.5 0.4 reshape.210
  195.1 2.1 gather_fusion.1
  197.1 0.2 gather.12
  197.3 1.6 multiply_reduce_fusion
  198.9 2.0 fusion.24
  (54 shorter events, 1.1 us)
Async XLA Ops:
  6.5 161.5 %copy-start = (bf16[1,1024,512]{2,1,0:T(8,128)(2,1)S(1)}, bf16[1,1024,512]{2,1,0:T(8,128)(2,1)}, u32[]{:S(2)}) copy-start(bf16[1,1024,512]{2,1,0:T(8,128)(2,1)} %param.28) | copy-start | bytes 3145732
  6.5 147.0 %all-gather.2.cloned.1.call-start = ((), (), s32[]{:S(2)}) async-start(), calls=%async_computation.2 | async-start | bytes 2457600 | tf_op jit(solution)/shard_map/all_gather | solution.py:105
  50.5 4.5 %copy-start.2 = (bf16[192,256]{1,0:T(8,128)(2,1)S(1)}, bf16[192,256]{1,0:T(8,128)(2,1)}, u32[]{:S(2)}) copy-start(bf16[192,256]{1,0:T(8,128)(2,1)} %param.19) | copy-start | bytes 294916
  87.4 4.1 %copy-start.5 = (f32[4]{0:T(128)S(1)}, f32[4]{0:T(128)}, u32[]{:S(2)}) copy-start(f32[4]{0:T(128)} %param.20) | copy-start | bytes 52
  87.4 4.2 %copy-start.7 = (f32[64]{0:T(128)S(1)}, f32[64]{0:T(128)}, u32[]{:S(2)}) copy-start(f32[64]{0:T(128)} %param.21) | copy-start | bytes 772
  87.4 11.6 %copy-start.9 = (bf16[1024,512]{1,0:T(8,128)(2,1)S(1)}, bf16[1024,512]{1,0:T(8,128)(2,1)}, u32[]{:S(2)}) copy-start(bf16[1024,512]{1,0:T(8,128)(2,1)} %param.22) | copy-start | bytes 3145732
  87.4 11.5 %copy-start.10 = (bf16[192,512]{1,0:T(8,128)(2,1)S(1)}, bf16[192,512]{1,0:T(8,128)(2,1)}, u32[]{:S(2)}) copy-start(bf16[192,512]{1,0:T(8,128)(2,1)} %param.16) | copy-start | bytes 589828
  91.4 17.7 %copy-start.4 = (f32[2048]{0:T(1024)S(1)}, f32[2048]{0:T(1024)}, u32[]{:S(2)}) copy-start(f32[2048]{0:T(1024)} %param.23) | copy-start | bytes 24580
  153.5 2.7 %copy-start.8 = (bf16[1,480,2048]{2,1,0:T(8,128)(2,1)S(1)}, bf16[1,480,2048]{2,1,0:T(8,128)(2,1)}, u32[]{:S(2)}) copy-start(bf16[1,480,2048]{2,1,0:T(8,128)(2,1)} %all-gather.2.cloned.1.call-done) | copy-start | bytes 5898244
  158.2 22.1 %copy-start.3 = (s32[192,2]{0,1:T(2,128)S(1)}, s32[192,2]{0,1:T(2,128)}, u32[]{:S(2)}) copy-start(s32[192,2]{0,1:T(2,128)} %param.24) | copy-start | bytes 4612
  158.2 22.2 %copy-start.6 = (f32[192,2]{0,1:T(2,128)S(1)}, f32[192,2]{0,1:T(2,128)}, u32[]{:S(2)}) copy-start(f32[192,2]{0,1:T(2,128)} %param.25) | copy-start | bytes 4612
  174.7 19.8 %all-to-all-start.1 = ((bf16[8,2,15360]{2,1,0:T(2,128)(2,1)}), bf16[8,2,15360]{2,1,0:T(2,128)(2,1)S(1)}, u32[]{:S(2)}, u32[]{:S(2)}) async-start(bf16[8,2,15360]{2,1,0:T(2,128)(2,1)} %reshape.209), calls=%async_computation.1 | async-start | bytes 983040 | tf_op jit(solution)/shard_map/all_to_all | solution.py:120
  195.1 3.9 %copy-start.1 = (bf16[1024,512]{1,0:T(8,128)(2,1)S(1)}, bf16[1024,512]{1,0:T(8,128)(2,1)}, u32[]{:S(2)}) copy-start(bf16[1024,512]{1,0:T(8,128)(2,1)} %param.31) | copy-start | bytes 3145732
Sparse Core Ops, SparseCore 0:
  133.3 20.2 all-gather.1
